TPU v7x, 1024 devices: a 2x16x16 block of a 4x16x16 slice. The times are simulated.
1024 devices in a mesh: grp: 2 (over x), sp: 16 (over z), tp: 32 (over y, core).
Axes of the slice: x: 2, y: 16, z: 16, core: 2. Of those that a mesh axis runs over, the one named last changes fastest.
The devices are a block of a 4x16x16 slice.
Arguments:
- grid_tokens: bfloat16 [256, 512, 1024], P(('grp', 'sp'), 'tp'), parts along dimension 0, may hold values from -6 to 6
- norm_gain: float32 [2, 1024], replicated, may hold values from 0.1 to 1.9
- w_query: bfloat16 [2, 1024, 512], replicated, may hold values from -0.84375 to 0.84375
- w_key: bfloat16 [2, 1024, 512], replicated, may hold values from -1.1390625 to 1.1390625
- w_value: bfloat16 [2, 1024, 512], replicated, may hold values from -0.1875 to 0.1875
- offset_bias: float32 [2, 4, 15, 31], replicated, may hold values from -5 to 5
- w_out: bfloat16 [2, 512, 1024], replicated, may hold values from -1 to 1
Outputs:
- grid_out: bfloat16 [256, 512, 1024], P(('grp', 'sp'), 'tp'), parts along dimension 0
There are 2 independent parts, one for each index of `grp`. A program takes and returns all parts, laid end to end along the dimension named above; an argument that names none is the same for every part. Nothing has to cross between parts.
All inputs are finite; a program needn't handle non-finite values.
Results may differ from a plain program's by a relative error of at most 0.014.
Values may be sent and summed in bfloat16 or wider, within the bound.
No kernel may reach another device: no remote copies, remote signals or barrier semaphores. Data moves between devices by JAX's collectives and lax.ppermute only.
A program may use at most 64 MiB of HBM per device.

v0:
```python
import jax
import jax.numpy as jnp
from jax import lax
from jax.sharding import PartitionSpec as P

HEAD_DIM = 128
WIN_ROWS = 8
WIN_COLS = 16
LAYERS = 2


NORM_EPSILON = 1e-06


def padded(cells, sides, width):
    for axis, dim in sides:
        count = lax.axis_size(axis)
        ends = count - 1
        head = lax.slice_in_dim(cells, 0, width, axis=dim)
        tail = lax.slice_in_dim(cells, cells.shape[dim] - width, cells.shape[dim], axis=dim)
        cells = jnp.concatenate(
            [
                lax.ppermute(tail, axis, [(i, (i + 1) % count) for i in range(ends)]),
                cells,
                lax.ppermute(head, axis, [((i + 1) % count, i) for i in range(ends)]),
            ],
            axis=dim,
        )
    return cells


def rms_rows(stream, gain):
    values = stream.astype(jnp.float32)
    factor = lax.rsqrt(jnp.mean(values * values, axis=-1, keepdims=True) + NORM_EPSILON)
    return (values * factor * gain).astype(jnp.bfloat16)


def project(normed, weight):
    return jnp.dot(normed, weight, preferred_element_type=jnp.float32).astype(jnp.bfloat16)


def add_branch(stream, mixture, weight):
    branch = jnp.dot(mixture, weight, preferred_element_type=jnp.float32)
    return (stream.astype(jnp.float32) + branch).astype(jnp.bfloat16)


def attend(
    queries,
    key_value,
    bias_table,
    query_row0,
    key_row0,
    col_shift,
    query_col0,
    grid_rows,
    grid_cols,
):
    query_rows, query_cols, inner = queries.shape
    head_count = bias_table.shape[0]
    inv_root = 1.0 / HEAD_DIM**0.5
    half_rows = WIN_ROWS // 2
    half_cols = WIN_COLS // 2
    slab_rows = WIN_ROWS + half_rows
    slab_cols = 2 * WIN_COLS

    def one_band(band_index):
        local_first = band_index * half_rows
        global_first = query_row0 + local_first
        row_ids = global_first + jnp.arange(half_rows, dtype=jnp.int32)
        slab_start = jnp.clip(global_first - half_rows, 0, grid_rows - slab_rows)
        slab = lax.dynamic_slice_in_dim(key_value, slab_start - key_row0, slab_rows, 1)
        slab_row_ids = slab_start + jnp.arange(slab_rows, dtype=jnp.int32)
        row_start = jnp.clip(row_ids - half_rows, 0, grid_rows - WIN_ROWS)
        row_inside = (slab_row_ids[None, :] >= row_start[:, None]) & (
            slab_row_ids[None, :] < row_start[:, None] + WIN_ROWS
        )
        row_offsets = jnp.clip(
            slab_row_ids[None, :] - row_ids[:, None] + WIN_ROWS - 1, 0, 2 * WIN_ROWS - 2
        )
        row_onehot = (
            row_offsets[:, :, None] == jnp.arange(2 * WIN_ROWS - 1, dtype=jnp.int32)[None, None, :]
        ).astype(jnp.float32)
        band_query = lax.dynamic_slice_in_dim(queries, local_first, half_rows, 0)
        outputs = []
        for offset in range(0, query_cols, WIN_COLS):
            first_key = offset + col_shift - half_cols
            keys_block = slab[:, :, first_key : first_key + slab_cols].reshape(
                2, slab_rows * slab_cols, head_count, HEAD_DIM
            )
            block_query = band_query[:, offset : offset + WIN_COLS].reshape(
                half_rows, WIN_COLS, head_count, HEAD_DIM
            )
            scores = (
                jnp.einsum(
                    "iqhd,khd->hiqk", block_query, keys_block[0], preferred_element_type=jnp.float32
                )
                * inv_root
            )
            query_col_ids = query_col0 + offset + jnp.arange(WIN_COLS, dtype=jnp.int32)
            key_col_ids = query_col0 + offset - half_cols + jnp.arange(slab_cols, dtype=jnp.int32)
            col_start = jnp.clip(query_col_ids - half_cols, 0, grid_cols - WIN_COLS)
            col_inside = (key_col_ids[None, :] >= col_start[:, None]) & (
                key_col_ids[None, :] < col_start[:, None] + WIN_COLS
            )
            col_offsets = jnp.clip(
                key_col_ids[None, :] - query_col_ids[:, None] + WIN_COLS - 1, 0, 2 * WIN_COLS - 2
            )
            col_onehot = (
                col_offsets[:, :, None]
                == jnp.arange(2 * WIN_COLS - 1, dtype=jnp.int32)[None, None, :]
            ).astype(jnp.float32)
            col_terms = jnp.einsum(
                "hab,qkb->haqk", bias_table, col_onehot, precision=lax.Precision.HIGHEST
            )
            offset_terms = jnp.einsum(
                "haqk,ija->hiqjk", col_terms, row_onehot, precision=lax.Precision.HIGHEST
            )
            offset_terms = offset_terms.reshape(
                head_count, half_rows, WIN_COLS, slab_rows * slab_cols
            )
            inside = (row_inside[:, None, :, None] & col_inside[None, :, None, :]).reshape(
                half_rows, WIN_COLS, slab_rows * slab_cols
            )
            scores = jnp.where(inside[None], scores + offset_terms, jnp.finfo(jnp.float32).min)
            top = jnp.max(scores, axis=3, keepdims=True)
            expo = jnp.exp(scores - top)
            attn_weights = (expo / jnp.sum(expo, axis=3, keepdims=True)).astype(jnp.bfloat16)
            mixture = jnp.einsum(
                "hiqk,khd->iqhd", attn_weights, keys_block[1], preferred_element_type=jnp.float32
            )
            outputs.append(mixture.astype(jnp.bfloat16).reshape(half_rows, WIN_COLS, inner))
        return jnp.concatenate(outputs, axis=1)

    pieces = lax.map(one_band, jnp.arange(query_rows // half_rows, dtype=jnp.int32))
    return pieces.reshape(query_rows, query_cols, inner)


def on_device(grid_tokens, norm_gain, w_query, w_key, w_value, offset_bias, w_out):
    tile_rows, tile_cols, model_width = grid_tokens.shape
    grid_rows = tile_rows * lax.axis_size("sp")
    grid_cols = tile_cols * lax.axis_size("tp")
    first_row = lax.axis_index("sp") * tile_rows
    first_col = lax.axis_index("tp") * tile_cols
    half_rows = WIN_ROWS // 2
    half_cols = WIN_COLS // 2
    stream = grid_tokens
    for layer_index in range(LAYERS):
        normed = rms_rows(stream, norm_gain[layer_index])
        queries = project(normed, w_query[layer_index])
        key_value = jnp.stack(
            (project(normed, w_key[layer_index]), project(normed, w_value[layer_index]))
        )
        key_value = padded(key_value, (("tp", 2),), half_cols)
        key_value = padded(key_value, (("sp", 1),), half_rows)
        mixture = attend(
            queries,
            key_value,
            offset_bias[layer_index],
            first_row,
            first_row - half_rows,
            half_cols,
            first_col,
            grid_rows,
            grid_cols,
        )
        stream = add_branch(stream, mixture, w_out[layer_index])
    return stream


def solution(mesh):
    return jax.shard_map(
        on_device,
        mesh=mesh,
        in_specs=(P(("grp", "sp"), "tp", None), P(), P(), P(), P(), P(), P()),
        out_specs=P(("grp", "sp"), "tp", None),
        check_vma=False,
    )
```

profile of v0, /device:TPU:5, one launch (start us, length us, event | category | flops | bytes accessed | tf_op | source)
XLA Modules:
  0.0 164.0 jit_solution(984197987992825399)
XLA Ops:
  0.0 0.8 fusion.73
  0.8 1.1 fusion.61
  1.9 1.7 %fusion.41 = bf16[1,8,16,512]{3,2,1,0:T(8,128)(2,1)S(1)} fusion(bf16[2,1024,512]{2,1,0:T(8,128)(2,1)} %param.14, bf16[8,16,1024]{2,1,0:T(8,128)(2,1)} %param.11, f32[1024]{0:T(1024)S(1)} %bitcast.192, f32[8,16]{1,0:T(8,128)S(1)} %add_rsqrt_fusion.1), kind=kOutput, calls=%fused_computation.93 | convolution fusion | flops 134807552 | bytes 1446400 | tf_op jit(solution)/shard_map/dot_general | solution.py:39
  3.6 1.6 fusion.42
  5.2 85.4 %collective-permute-start.1 = (bf16[2,8,8,512]{3,2,1,0:T(8,128)(2,1)S(1)}, bf16[2,8,8,512]{3,2,1,0:T(8,128)(2,1)S(1)}, u32[]{:S(2)}, u32[]{:S(2)}) collective-permute-start(bf16[2,8,8,512]{3,2,1,0:T(8,128)(2,1)S(1)} %get-tuple-element.528), channel_id=1, source_target_pairs={{1,0},{2,1},{3,2},{4,3},{5,4},{6,5},{7,6},{8,7},{9,8},{10,9},{11,1... | collective-permute-start | bytes 393224 | tf_op jit(solution)/shard_map/ppermute | solution.py:25
  90.6 2.0 %collective-permute-start = (bf16[2,8,8,512]{3,2,1,0:T(8,128)(2,1)S(1)}, bf16[2,8,8,512]{3,2,1,0:T(8,128)(2,1)S(1)}, u32[]{:S(2)}, u32[]{:S(2)}) collective-permute-start(bf16[2,8,8,512]{3,2,1,0:T(8,128)(2,1)S(1)} %get-tuple-element.527), channel_id=1, source_target_pairs={{0,1},{1,2},{2,3},{3,4},{4,5},{5,6},{6,7},{7,8},{8,9},{9,10},{10,1... | collective-permute-start | bytes 393224 | tf_op jit(solution)/shard_map/ppermute | solution.py:23
  92.6 1.9 %collective-permute-done = bf16[2,8,8,512]{3,2,1,0:T(8,128)(2,1)S(1)} collective-permute-done((bf16[2,8,8,512]{3,2,1,0:T(8,128)(2,1)S(1)}, bf16[2,8,8,512]{3,2,1,0:T(8,128)(2,1)S(1)}, u32[]{:S(2)}, u32[]{:S(2)}) %collective-permute-start) | collective-permute-done | bytes 131104 | tf_op jit(solution)/shard_map/ppermute | solution.py:23
  94.6 1.3 collective-permute-start.3
  95.9 4.0 %collective-permute-start.2 = (bf16[2,4,32,512]{3,2,1,0:T(8,128)(2,1)S(1)}, bf16[2,4,32,512]{3,2,1,0:T(8,128)(2,1)S(1)}, u32[]{:S(2)}, u32[]{:S(2)}) collective-permute-start(bf16[2,4,32,512]{3,2,1,0:T(8,128)(2,1)S(1)} %get-tuple-element.523), channel_id=1, source_target_pairs={{0,32},{32,64},{64,96},{96,128},{128,160},{160,192},{192,224},{224... | collective-permute-start | bytes 786440 | tf_op jit(solution)/shard_map/ppermute | solution.py:23
  100.0 1.6 convolution_convert_fusion.5
  101.6 3.3 %collective-permute-done.3 = bf16[2,4,32,512]{3,2,1,0:T(8,128)(2,1)S(1)} collective-permute-done((bf16[2,4,32,512]{3,2,1,0:T(8,128)(2,1)S(1)}, bf16[2,4,32,512]{3,2,1,0:T(8,128)(2,1)S(1)}, u32[]{:S(2)}, u32[]{:S(2)}) %collective-permute-start.3) | collective-permute-done | bytes 262176 | tf_op jit(solution)/shard_map/ppermute | solution.py:25
  104.8 0.9 collective-permute-done.2
  105.8 1.1 pad_maximum_fusion
  106.8 0.7 broadcast.1091.clone
  107.5 15.4 %while.30 = (s32[]{:T(128)}, bf16[2,4,16,512]{3,2,1,0:T(8,128)(2,1)}, s32[2]{0:T(128)S(1)}, s32[]{:T(128)}, s32[]{:T(128)}, /*index=5*/bf16[2,16,32,512]{3,2,1,0...) while((s32[]{:T(128)}, ...), condition=%wide.region_4.5_spmd, body=%wide.region_1.4_spmd.sunk | while | flops 80319152 | bytes 8599697 | solution.py:134
  107.5 0.6 dynamic_slice.72
  108.8 1.2 constant_dynamic-slice_fusion.6
  110.1 0.8 convolution_bitcast_fusion.8
  111.1 1.0 convolution_bitcast_fusion.9
  112.1 0.6 reshape.568
  113.3 0.3 fusion.118
  113.8 0.6 fusion.120
  114.6 0.6 copy-done.5
  115.2 0.6 dynamic_slice.72
  116.4 1.2 constant_dynamic-slice_fusion.6
  117.8 0.8 convolution_bitcast_fusion.8
  118.8 1.0 convolution_bitcast_fusion.9
  119.8 0.6 reshape.568
  121.0 0.3 fusion.118
  121.5 0.6 fusion.120
  122.2 0.6 copy-done.5
  122.9 1.8 %multiply_reduce_fusion = (f32[8,16]{1,0:T(8,128)S(1)}, f32[8,16,1024]{2,1,0:T(8,128)S(1)}) fusion(bf16[8,16,512]{2,1,0:T(8,128)(2,1)} %bitcast.190, bf16[2,512,1024]{2,1,0:T(8,128)(2,1)} %param.17, bf16[8,16,1024]{2,1,0:T(8,128)(2,1)} %param.11), kind=kOutput, calls=%fused_computation.123 | convolution fusion | flops 135004032 | bytes 1966592 | tf_op jit(solution)/shard_map/dot_general | solution.py:43
  124.9 0.3 fusion.43
  125.2 0.3 copy-done.8
  125.5 0.3 fusion.44
  125.9 2.6 %collective-permute-start.5 = (bf16[2,8,8,512]{3,2,1,0:T(8,128)(2,1)S(1)}, bf16[2,8,8,512]{3,2,1,0:T(8,128)(2,1)S(1)}, u32[]{:S(2)}, u32[]{:S(2)}) collective-permute-start(bf16[2,8,8,512]{3,2,1,0:T(8,128)(2,1)S(1)} %get-tuple-element.526), channel_id=1, source_target_pairs={{1,0},{2,1},{3,2},{4,3},{5,4},{6,5},{7,6},{8,7},{9,8},{10,9},{11,1... | collective-permute-start | bytes 393224 | tf_op jit(solution)/shard_map/ppermute | solution.py:25
  128.5 3.0 %collective-permute-start.4 = (bf16[2,8,8,512]{3,2,1,0:T(8,128)(2,1)S(1)}, bf16[2,8,8,512]{3,2,1,0:T(8,128)(2,1)S(1)}, u32[]{:S(2)}, u32[]{:S(2)}) collective-permute-start(bf16[2,8,8,512]{3,2,1,0:T(8,128)(2,1)S(1)} %get-tuple-element.525), channel_id=1, source_target_pairs={{0,1},{1,2},{2,3},{3,4},{4,5},{5,6},{6,7},{7,8},{8,9},{9,10},{10,1... | collective-permute-start | bytes 393224 | tf_op jit(solution)/shard_map/ppermute | solution.py:23
  131.5 0.7 collective-permute-done.5
  132.2 1.2 collective-permute-done.4
  133.6 1.3 collective-permute-start.7
  134.9 4.8 %collective-permute-start.6 = (bf16[2,4,32,512]{3,2,1,0:T(8,128)(2,1)S(1)}, bf16[2,4,32,512]{3,2,1,0:T(8,128)(2,1)S(1)}, u32[]{:S(2)}, u32[]{:S(2)}) collective-permute-start(bf16[2,4,32,512]{3,2,1,0:T(8,128)(2,1)S(1)} %get-tuple-element.521), channel_id=1, source_target_pairs={{0,32},{32,64},{64,96},{96,128},{128,160},{160,192},{192,224},{224... | collective-permute-start | bytes 786440 | tf_op jit(solution)/shard_map/ppermute | solution.py:23
  139.7 1.5 convolution_convert_fusion.2
  141.2 1.7 %collective-permute-done.7 = bf16[2,4,32,512]{3,2,1,0:T(8,128)(2,1)S(1)} collective-permute-done((bf16[2,4,32,512]{3,2,1,0:T(8,128)(2,1)S(1)}, bf16[2,4,32,512]{3,2,1,0:T(8,128)(2,1)S(1)}, u32[]{:S(2)}, u32[]{:S(2)}) %collective-permute-start.7) | collective-permute-done | bytes 262176 | tf_op jit(solution)/shard_map/ppermute | solution.py:25
  142.9 1.8 %collective-permute-done.6 = bf16[2,4,32,512]{3,2,1,0:T(8,128)(2,1)S(1)} collective-permute-done((bf16[2,4,32,512]{3,2,1,0:T(8,128)(2,1)S(1)}, bf16[2,4,32,512]{3,2,1,0:T(8,128)(2,1)S(1)}, u32[]{:S(2)}, u32[]{:S(2)}) %collective-permute-start.6) | collective-permute-done | bytes 262176 | tf_op jit(solution)/shard_map/ppermute | solution.py:23
  144.7 1.1 pad_maximum_fusion.1
  145.8 0.7 broadcast.1091
  146.5 15.1 %while.31 = (s32[]{:T(128)}, bf16[2,4,16,512]{3,2,1,0:T(8,128)(2,1)}, s32[2]{0:T(128)S(1)}, s32[]{:T(128)}, s32[]{:T(128)}, /*index=5*/bf16[2,16,32,512]{3,2,1,0...) while((s32[]{:T(128)}, ...), condition=%wide.region_9.10_spmd, body=%wide.region_6.9_spmd.sunk | while | flops 80319152 | bytes 8599697 | solution.py:134
  146.5 0.5 dynamic_slice.74
  147.6 1.2 constant_dynamic-slice_fusion.7
  149.0 0.8 convolution_bitcast_fusion.10
  149.9 1.0 convolution_bitcast_fusion.11
  150.9 0.6 reshape.569
  152.1 0.3 fusion.130
  152.7 0.6 fusion.132
  153.4 0.6 copy-done.3
  154.0 0.5 dynamic_slice.74
  155.1 1.2 constant_dynamic-slice_fusion.7
  156.5 0.8 convolution_bitcast_fusion.10
  157.4 1.0 convolution_bitcast_fusion.11
  158.5 0.6 reshape.569
  159.7 0.3 fusion.130
  160.2 0.6 fusion.132
  160.9 0.6 copy-done.3
  161.6 2.4 %fusion.40 = bf16[8,16,1024]{2,1,0:T(8,128)(2,1)} fusion(f32[8,16,1024]{2,1,0:T(8,128)} %copy-done, bf16[8,16,512]{2,1,0:T(8,128)(2,1)} %bitcast.189, bf16[2,512,1024]{2,1,0:T(8,128)(2,1)} %param.17), kind=kOutput, calls=%fused_computation.86 | convolution fusion | flops 134479872 | bytes 1966080 | tf_op jit(solution)/shard_map/dot_general | solution.py:43
  (118 shorter events, 5.1 us)
Async XLA Ops:
  0.0 3.5 %copy-start.1 = (bf16[8,16,1024]{2,1,0:T(8,128)(2,1)S(1)}, bf16[8,16,1024]{2,1,0:T(8,128)(2,1)}, u32[]{:S(2)}) copy-start(bf16[8,16,1024]{2,1,0:T(8,128)(2,1)} %param.11) | copy-start | bytes 786436
  3.6 96.4 %copy-start.6 = (f32[2,4,15,31]{3,1,2,0:T(4,128)S(1)}, f32[2,4,15,31]{3,1,2,0:T(4,128)}, u32[]{:S(2)}) copy-start(f32[2,4,15,31]{3,1,2,0:T(4,128)} %param.16) | copy-start | bytes 44644
  5.2 87.4 %collective-permute-start.1 = (bf16[2,8,8,512]{3,2,1,0:T(8,128)(2,1)S(1)}, bf16[2,8,8,512]{3,2,1,0:T(8,128)(2,1)S(1)}, u32[]{:S(2)}, u32[]{:S(2)}) collective-permute-start(bf16[2,8,8,512]{3,2,1,0:T(8,128)(2,1)S(1)} %get-tuple-element.528), channel_id=1, source_target_pairs={{1,0},{2,1},{3,2},{4,3},{5,4},{6,5},{7,6},{8,7},{9,8},{10,9},{11,1... | collective-permute-start | bytes 393224 | tf_op jit(solution)/shard_map/ppermute | solution.py:25
  90.6 3.9 %collective-permute-start = (bf16[2,8,8,512]{3,2,1,0:T(8,128)(2,1)S(1)}, bf16[2,8,8,512]{3,2,1,0:T(8,128)(2,1)S(1)}, u32[]{:S(2)}, u32[]{:S(2)}) collective-permute-start(bf16[2,8,8,512]{3,2,1,0:T(8,128)(2,1)S(1)} %get-tuple-element.527), channel_id=1, source_target_pairs={{0,1},{1,2},{2,3},{3,4},{4,5},{5,6},{6,7},{7,8},{8,9},{9,10},{10,1... | collective-permute-start | bytes 393224 | tf_op jit(solution)/shard_map/ppermute | solution.py:23
  94.6 10.2 %collective-permute-start.3 = (bf16[2,4,32,512]{3,2,1,0:T(8,128)(2,1)S(1)}, bf16[2,4,32,512]{3,2,1,0:T(8,128)(2,1)S(1)}, u32[]{:S(2)}, u32[]{:S(2)}) collective-permute-start(bf16[2,4,32,512]{3,2,1,0:T(8,128)(2,1)S(1)} %get-tuple-element.524), channel_id=1, source_target_pairs={{32,0},{64,32},{96,64},{128,96},{160,128},{192,160},{224,192},{256... | collective-permute-start | bytes 786440 | tf_op jit(solution)/shard_map/ppermute | solution.py:25
  95.9 9.9 %collective-permute-start.2 = (bf16[2,4,32,512]{3,2,1,0:T(8,128)(2,1)S(1)}, bf16[2,4,32,512]{3,2,1,0:T(8,128)(2,1)S(1)}, u32[]{:S(2)}, u32[]{:S(2)}) collective-permute-start(bf16[2,4,32,512]{3,2,1,0:T(8,128)(2,1)S(1)} %get-tuple-element.523), channel_id=1, source_target_pairs={{0,32},{32,64},{64,96},{96,128},{128,160},{160,192},{192,224},{224... | collective-permute-start | bytes 786440 | tf_op jit(solution)/shard_map/ppermute | solution.py:23
  113.1 1.4 copy-start.4
  114.5 0.7 copy-start.5
  120.8 1.4 copy-start.4
  122.2 0.7 copy-start.5
  122.9 2.0 %copy-start.7 = (bf16[2,1024,512]{2,1,0:T(8,128)(2,1)S(1)}, bf16[2,1024,512]{2,1,0:T(8,128)(2,1)}, u32[]{:S(2)}) copy-start(bf16[2,1024,512]{2,1,0:T(8,128)(2,1)} %param.14) | copy-start | bytes 6291460
  122.9 2.7 %copy-start.8 = (bf16[2,1024,512]{2,1,0:T(8,128)(2,1)S(1)}, bf16[2,1024,512]{2,1,0:T(8,128)(2,1)}, u32[]{:S(2)}) copy-start(bf16[2,1024,512]{2,1,0:T(8,128)(2,1)} %param.15) | copy-start | bytes 6291460
  124.7 1.2 copy-start
  125.9 6.3 %collective-permute-start.5 = (bf16[2,8,8,512]{3,2,1,0:T(8,128)(2,1)S(1)}, bf16[2,8,8,512]{3,2,1,0:T(8,128)(2,1)S(1)}, u32[]{:S(2)}, u32[]{:S(2)}) collective-permute-start(bf16[2,8,8,512]{3,2,1,0:T(8,128)(2,1)S(1)} %get-tuple-element.526), channel_id=1, source_target_pairs={{1,0},{2,1},{3,2},{4,3},{5,4},{6,5},{7,6},{8,7},{9,8},{10,9},{11,1... | collective-permute-start | bytes 393224 | tf_op jit(solution)/shard_map/ppermute | solution.py:25
  128.5 5.0 %collective-permute-start.4 = (bf16[2,8,8,512]{3,2,1,0:T(8,128)(2,1)S(1)}, bf16[2,8,8,512]{3,2,1,0:T(8,128)(2,1)S(1)}, u32[]{:S(2)}, u32[]{:S(2)}) collective-permute-start(bf16[2,8,8,512]{3,2,1,0:T(8,128)(2,1)S(1)} %get-tuple-element.525), channel_id=1, source_target_pairs={{0,1},{1,2},{2,3},{3,4},{4,5},{5,6},{6,7},{7,8},{8,9},{9,10},{10,1... | collective-permute-start | bytes 393224 | tf_op jit(solution)/shard_map/ppermute | solution.py:23
  133.6 9.4 %collective-permute-start.7 = (bf16[2,4,32,512]{3,2,1,0:T(8,128)(2,1)S(1)}, bf16[2,4,32,512]{3,2,1,0:T(8,128)(2,1)S(1)}, u32[]{:S(2)}, u32[]{:S(2)}) collective-permute-start(bf16[2,4,32,512]{3,2,1,0:T(8,128)(2,1)S(1)} %get-tuple-element.522), channel_id=1, source_target_pairs={{32,0},{64,32},{96,64},{128,96},{160,128},{192,160},{224,192},{256... | collective-permute-start | bytes 786440 | tf_op jit(solution)/shard_map/ppermute | solution.py:25
  134.9 9.8 %collective-permute-start.6 = (bf16[2,4,32,512]{3,2,1,0:T(8,128)(2,1)S(1)}, bf16[2,4,32,512]{3,2,1,0:T(8,128)(2,1)S(1)}, u32[]{:S(2)}, u32[]{:S(2)}) collective-permute-start(bf16[2,4,32,512]{3,2,1,0:T(8,128)(2,1)S(1)} %get-tuple-element.521), channel_id=1, source_target_pairs={{0,32},{32,64},{64,96},{96,128},{128,160},{160,192},{192,224},{224... | collective-permute-start | bytes 786440 | tf_op jit(solution)/shard_map/ppermute | solution.py:23
  151.9 1.4 copy-start.2
  153.4 0.7 copy-start.3
  159.5 1.4 copy-start.2
  160.9 0.7 copy-start.3
where the time goes:
time: 165 us; the launch traced here: 164 us
  starting transfers between devices  104 us (63%)
  matrix products  22.1 us (13%)
  local copies, waits for them, and re-layouts  17 us (10%)
  waiting for transfers between devices  11.5 us (7%)
  other arithmetic  5.78 us (4%)
  loops' own time  2.95 us (2%)
    ppermute x4, starting transfers between devices, padded(): lax.ppermute(head, axis, [((i + 1) % count, i) for i in range(ends)])  90.6 us
    ppermute x4, starting transfers between devices, padded(): lax.ppermute(tail, axis, [(i, (i + 1) % count) for i in range(ends)])  13.8 us
    dot_general x6, matrix products, project(): jnp.dot(normed, weight, preferred_element_type=jnp.float32)  6.98 us
    ppermute x4, waiting for transfers between devices, padded(): lax.ppermute(tail, axis, [(i, (i + 1) % count) for i in range(ends)])  5.89 us
    ppermute x4, waiting for transfers between devices, padded(): lax.ppermute(head, axis, [((i + 1) % count, i) for i in range(ends)])  5.63 us
    slice x4, local copies, waits for them, and re-layouts, one_band(): keys_block[0]  4.7 us
    dot_general x2, matrix products, add_branch(): branch = jnp.dot(mixture, weight, preferred_element_type=jnp.float32)  4.25 us
    dot_general x4, matrix products, one_band(): jnp.einsum('haqk,ija->hiqjk', col_terms, row_onehot, precision=lax.Precis...  4.11 us
  transfers between devices with their start and end apart: 8, of which 7 were waited for; matrix products, arithmetic and copies ran while one was open for 2% of the time, Pallas kernels for 0%

commit v1 on v0

v1 whole, which is shorter than its diff:
```python
import functools
import math

import jax
import jax.numpy as jnp
from jax import lax
from jax.experimental import pallas as pl
from jax.experimental.pallas import tpu as pltpu
from jax.sharding import PartitionSpec as P

HEAD_DIM = 128
WIN_ROWS = 8
WIN_COLS = 16
LAYERS = 2
HALF_ROWS = WIN_ROWS // 2
HALF_COLS = WIN_COLS // 2

NORM_EPSILON = 1e-06
LOG2E = math.log2(math.e)
MASKED = -1e30

BLOCK_ROWS = 8
BLOCK_COLS = 16
SLAB_ROWS = BLOCK_ROWS + WIN_ROWS
SLAB_COLS = BLOCK_COLS + WIN_COLS
QUERIES = BLOCK_ROWS * BLOCK_COLS
SLAB = SLAB_ROWS * SLAB_COLS
LANES = 128
GROUP = LANES // SLAB_COLS
SPAN = SLAB_ROWS - GROUP + BLOCK_ROWS
BLOCKS = 5

VMEM = pl.BlockSpec(memory_space=pltpu.VMEM)


def bias_rows(table):
    before = HALF_ROWS
    after = SPAN + GROUP - 1 - before - table.shape[2]
    rows = jnp.pad(
        table * LOG2E, ((0, 0), (0, 0), (before, after), (0, SLAB_COLS - table.shape[3]))
    )
    return jnp.concatenate([rows[:, :, g : g + SPAN] for g in range(GROUP)], axis=3)


def bias_kernel(grid_rows, grid_cols, tile_rows, tile_cols, rows_ref, out_ref, shifted):
    layers, heads = rows_ref.shape[:2]
    first_row = lax.axis_index("sp") * tile_rows
    first_col = lax.axis_index("tp") * tile_cols

    def shift(index, _):
        layer, head = index // heads, index % heads
        for u in range(SPAN):
            line = jnp.broadcast_to(rows_ref[layer, head, u : u + 1], (BLOCK_COLS, LANES))
            shifted[layer, head, u] = pltpu.roll(
                line, LANES - (HALF_COLS - 1), 1, stride=1, stride_axis=0
            )
        return 0

    lax.fori_loop(0, layers * heads, shift, 0)
    lane = lax.broadcasted_iota(jnp.int32, (BLOCK_COLS, LANES), 1)
    column = lax.broadcasted_iota(jnp.int32, (BLOCK_COLS, LANES), 0)
    key_col = lane % SLAB_COLS
    key_row = lane // SLAB_COLS

    def block(index, _):
        last = index // (BLOCKS - 1)
        row_block, col_block = (index // 2) % 2, index % 2
        row0 = first_row + (1 - last) * (row_block * BLOCK_ROWS - HALF_ROWS)
        col0 = first_col + (1 - last) * (col_block * BLOCK_COLS - HALF_COLS)
        col_start = jnp.clip(col0 + column - HALF_COLS, 0, grid_cols - WIN_COLS)
        behind = col0 - HALF_COLS + key_col - col_start
        col_inside = (behind >= 0) & (behind < WIN_COLS)
        for i in range(BLOCK_ROWS):
            row_start = jnp.clip(row0 + i - HALF_ROWS, 0, grid_rows - WIN_ROWS)
            for j in range(SLAB_ROWS // GROUP):
                below = key_row + (row0 - HALF_ROWS + j * GROUP - row_start)
                inside = col_inside & (below >= 0) & (below < WIN_ROWS)
                for head in range(heads):
                    out_ref[
                        index,
                        head,
                        i * BLOCK_COLS : (i + 1) * BLOCK_COLS,
                        j * LANES : (j + 1) * LANES,
                    ] = jnp.where(
                        inside, shifted[last, head, GROUP * j - i + BLOCK_ROWS - 1], MASKED
                    )
        return 0

    lax.fori_loop(0, BLOCKS, block, 0)


def normed_rows(values, gain):
    factor = lax.rsqrt(jnp.mean(values * values, axis=-1, keepdims=True) + NORM_EPSILON)
    return values * factor * gain


def project(cells, weight):
    rows, cols, width = cells.shape
    out = jnp.dot(
        cells.reshape(rows * cols, width), weight, preferred_element_type=jnp.float32
    )
    return out.astype(jnp.bfloat16).reshape(rows, cols, weight.shape[1])


def attend(queries, keys, values, bias):
    scores = lax.dot_general(
        queries.reshape(QUERIES, HEAD_DIM),
        keys.reshape(SLAB, HEAD_DIM),
        (((1,), (1,)), ((), ())),
        preferred_element_type=jnp.float32,
    )
    scores = scores * (LOG2E / HEAD_DIM**0.5) + bias
    expo = jnp.exp2(scores - jnp.max(scores, axis=1, keepdims=True))
    total = jnp.sum(expo, axis=1, keepdims=True)
    mixture = jnp.dot(
        expo.astype(jnp.bfloat16),
        values.reshape(SLAB, HEAD_DIM),
        preferred_element_type=jnp.float32,
    )
    return (mixture / total).astype(jnp.bfloat16).reshape(BLOCK_ROWS, BLOCK_COLS, HEAD_DIM)


def layers_kernel(
    left,
    mid,
    right,
    gain,
    w_query,
    w_key,
    w_value,
    w_out,
    bias,
    out_ref,
    normed,
    normed_q,
    keys,
    values,
    queries,
    mixture,
    branch,
    center,
):
    f32, bf16 = jnp.float32, jnp.bfloat16
    heads = w_query.shape[2] // HEAD_DIM
    region_rows, region_cols = mixture.shape[:2]

    def norm_first(r, _):
        parts = [normed_rows(ref[r].astype(f32), gain[0:1]) for ref in (left, mid, right)]
        for index, part in enumerate(parts):
            normed[r, index * BLOCK_COLS : (index + 1) * BLOCK_COLS] = part.astype(bf16)
        for index in range(2):
            both = (parts[index][HALF_COLS:], parts[index + 1][:HALF_COLS])
            normed_q[r, index * BLOCK_COLS : (index + 1) * BLOCK_COLS] = jnp.concatenate(
                both, axis=0
            ).astype(bf16)
        return 0

    lax.fori_loop(0, left.shape[0], norm_first, 0)
    keys[...] = project(normed[...], w_key[0])
    values[...] = project(normed[...], w_value[0])
    queries[...] = project(normed_q[HALF_ROWS : HALF_ROWS + region_rows], w_query[0])

    def first_block(index, _):
        row = index // 2 * BLOCK_ROWS
        col = pl.multiple_of(index % 2 * BLOCK_COLS, BLOCK_COLS)
        tile = (pl.ds(row, BLOCK_ROWS), pl.ds(col, BLOCK_COLS))
        slab = (pl.ds(row, SLAB_ROWS), pl.ds(col, SLAB_COLS))
        for head in range(heads):
            lanes = pl.ds(head * HEAD_DIM, HEAD_DIM)
            mixture[(*tile, lanes)] = attend(
                queries[(*tile, lanes)],
                keys[(*slab, lanes)],
                values[(*slab, lanes)],
                bias[index, head],
            )
        return 0

    lax.fori_loop(0, BLOCKS - 1, first_block, 0)
    branch[...] = jnp.dot(
        mixture[...].reshape(region_rows * region_cols, heads * HEAD_DIM),
        w_out[0],
        preferred_element_type=f32,
    ).reshape(branch.shape)

    def norm_second(r, _):
        tokens = jnp.concatenate(
            (
                left[r + HALF_ROWS].astype(f32)[HALF_COLS:],
                mid[r + HALF_ROWS].astype(f32),
                right[r + HALF_ROWS].astype(f32)[:HALF_COLS],
            ),
            axis=0,
        )
        stream = (tokens + branch[r]).astype(bf16).astype(f32)
        part = normed_rows(stream, gain[1:2])
        normed[r, :region_cols] = part.astype(bf16)
        normed_q[r, :BLOCK_COLS] = part[HALF_COLS : HALF_COLS + BLOCK_COLS].astype(bf16)
        center[r] = stream[HALF_COLS : HALF_COLS + BLOCK_COLS]
        return 0

    lax.fori_loop(0, region_rows, norm_second, 0)
    own = pl.ds(HALF_ROWS, BLOCK_ROWS)
    keys[:region_rows, :region_cols] = project(normed[:region_rows, :region_cols], w_key[1])
    values[:region_rows, :region_cols] = project(normed[:region_rows, :region_cols], w_value[1])
    queries[:BLOCK_ROWS, :BLOCK_COLS] = project(normed_q[own, :BLOCK_COLS], w_query[1])
    for head in range(heads):
        lanes = pl.ds(head * HEAD_DIM, HEAD_DIM)
        mixture[:BLOCK_ROWS, :BLOCK_COLS, lanes] = attend(
            queries[:BLOCK_ROWS, :BLOCK_COLS, lanes],
            keys[:SLAB_ROWS, :SLAB_COLS, lanes],
            values[:SLAB_ROWS, :SLAB_COLS, lanes],
            bias[BLOCKS - 1, head],
        )
    last = jnp.dot(
        mixture[:BLOCK_ROWS, :BLOCK_COLS].reshape(QUERIES, heads * HEAD_DIM),
        w_out[1],
        preferred_element_type=f32,
    )
    out_ref[...] = (center[own] + last.reshape(out_ref.shape)).astype(out_ref.dtype)


def shifts(cells, axis):
    ends = lax.axis_size(axis) - 1
    before = lax.ppermute(cells, axis, [(i, i + 1) for i in range(ends)])
    after = lax.ppermute(cells, axis, [(i + 1, i) for i in range(ends)])
    return before, after


def on_device(grid_tokens, norm_gain, w_query, w_key, w_value, offset_bias, w_out):
    tile_rows, tile_cols, width = grid_tokens.shape
    grid_rows = tile_rows * lax.axis_size("sp")
    grid_cols = tile_cols * lax.axis_size("tp")
    heads = offset_bias.shape[1]
    inner = heads * HEAD_DIM
    bf16, f32 = jnp.bfloat16, jnp.float32

    bias = pl.pallas_call(
        functools.partial(bias_kernel, grid_rows, grid_cols, tile_rows, tile_cols),
        out_shape=jax.ShapeDtypeStruct((BLOCKS, heads, QUERIES, SLAB), f32),
        in_specs=[VMEM],
        out_specs=VMEM,
        scratch_shapes=[pltpu.VMEM((LAYERS, heads, SPAN, BLOCK_COLS, LANES), f32)],
        compiler_params=pltpu.CompilerParams(vmem_limit_bytes=16 * 2**20),
        cost_estimate=pl.CostEstimate(flops=4 * 10**6, bytes_accessed=6 * 2**20, transcendentals=0),
        name="bias",
    )(bias_rows(offset_bias))

    above, below = shifts(grid_tokens, "sp")
    column = jnp.concatenate((above, grid_tokens, below), axis=0)
    left, right = shifts(column, "tp")

    rows, cols = 3 * tile_rows, 3 * tile_cols
    region_rows, region_cols = 2 * tile_rows, 2 * tile_cols
    return pl.pallas_call(
        layers_kernel,
        out_shape=jax.ShapeDtypeStruct(grid_tokens.shape, grid_tokens.dtype),
        in_specs=[VMEM] * 9,
        out_specs=VMEM,
        scratch_shapes=[
            pltpu.VMEM((rows, cols, width), bf16),
            pltpu.VMEM((rows, region_cols, width), bf16),
            pltpu.VMEM((rows, cols, inner), bf16),
            pltpu.VMEM((rows, cols, inner), bf16),
            pltpu.VMEM((region_rows, region_cols, inner), bf16),
            pltpu.VMEM((region_rows, region_cols, inner), bf16),
            pltpu.VMEM((region_rows, region_cols, width), f32),
            pltpu.VMEM((region_rows, tile_cols, width), f32),
        ],
        compiler_params=pltpu.CompilerParams(vmem_limit_bytes=40 * 2**20),
        cost_estimate=pl.CostEstimate(
            flops=6 * 10**9, bytes_accessed=16 * 2**20, transcendentals=10**6
        ),
        name="layers",
    )(left, column, right, norm_gain, w_query, w_key, w_value, w_out, bias)


def solution(mesh):
    return jax.shard_map(
        on_device,
        mesh=mesh,
        in_specs=(P(("grp", "sp"), "tp", None), P(), P(), P(), P(), P(), P()),
        out_specs=P(("grp", "sp"), "tp", None),
        check_vma=False,
    )
```

time: 165 us -> 127 us (0.77)
  matrix products: 22.1 us -> 0 us
  Pallas kernels: 0 us -> 20.8 us
  starting transfers between devices: 104 us -> 86.2 us
  local copies, waits for them, and re-layouts: 17 us -> 4.94 us
  other arithmetic: 5.78 us -> 0.99 us
  loops' own time: 2.95 us -> 0 us
  waiting for transfers between devices: 11.5 us -> 14 us
    dot_general x24 -> x0, matrix products: 22.1 us -> none  [the longest x6 6.98 us: project(): jnp.dot(normed, weight, preferred_element_type=jnp.float32)]
    pallas_call x0 -> x2, Pallas kernels: none -> 20.8 us  [the longest x1 19.3 us: on_device(): pl.pallas_call(layers_kernel, out_shape=jax.ShapeDtypeStruct(grid_tokens....]
    ppermute x8 -> x4, starting transfers between devices: 104 us -> 86.2 us  [the longest x2 75 us: shifts(): after = lax.ppermute(cells, axis, [(i + 1, i) for i in range(ends)])]
    slice x7 -> x1, local copies, waits for them, and re-layouts: 5.56 us -> 0.04 us  [bias_rows(): rows[:, :, g:g + SPAN]]
    unnamed x10 -> x14, local copies, waits for them, and re-layouts: 0.37 us -> 4.89 us
    another operation x2 -> x0, loops' own time: 2.95 us -> none  [attend(): lax.map(one_band, jnp.arange(query_rows // half_rows, dtype=jnp.int32))]
    while x16 -> x0, local copies, waits for them, and re-layouts: 2.62 us -> none
    ppermute x8 -> x4, waiting for transfers between devices: 11.5 us -> 14 us  [the longest x2 7.74 us: shifts(): after = lax.ppermute(cells, axis, [(i + 1, i) for i in range(ends)])]
  transfers between devices with their start and end apart: 8 -> 4, of which waited for: 7 -> 3; matrix products, arithmetic and copies ran while one was open for 2% -> 2% of each run, Pallas kernels for 0% -> 1%
where the time goes in v1:
time: 127 us
  starting transfers between devices  86.2 us (68%)
  Pallas kernels  20.8 us (16%)
  waiting for transfers between devices  14 us (11%)
  local copies, waits for them, and re-layouts  4.94 us (4%)
    ppermute x2, starting transfers between devices, shifts(): after = lax.ppermute(cells, axis, [(i + 1, i) for i in range(ends)])  75 us
    pallas_call x1, Pallas kernels, on_device(): pl.pallas_call(layers_kernel, out_shape=jax.ShapeDtypeStruct(grid_tokens....  19.3 us
    ppermute x2, starting transfers between devices, shifts(): before = lax.ppermute(cells, axis, [(i, i + 1) for i in range(ends)])  11.1 us
    ppermute x2, waiting for transfers between devices, shifts(): after = lax.ppermute(cells, axis, [(i + 1, i) for i in range(ends)])  7.74 us
    ppermute x2, waiting for transfers between devices, shifts(): before = lax.ppermute(cells, axis, [(i, i + 1) for i in range(ends)])  6.3 us
    unnamed x14, local copies, waits for them, and re-layouts  4.89 us
  transfers between devices with their start and end apart: 4, of which 3 were waited for; matrix products, arithmetic and copies ran while one was open for 2% of the time, Pallas kernels for 1%

profile of v1, /device:TPU:5, one launch (start us, length us, event | category | flops | bytes accessed | tf_op | source)
XLA Modules:
  0.0 127.0 jit_solution(12354061601872725827)
XLA Ops:
  0.0 9.2 %collective-permute-start = (bf16[8,16,1024]{2,1,0:T(8,128)(2,1)}, bf16[8,16,1024]{2,1,0:T(8,128)(2,1)S(1)}, u32[]{:S(2)}, u32[]{:S(2)}) collective-permute-start(bf16[8,16,1024]{2,1,0:T(8,128)(2,1)} %param.7), channel_id=1, source_target_pairs={{0,32},{32,64},{64,96},{96,128},{128,160},{160,192},{192,224},{224... | collective-permute-start | bytes 786440 | tf_op jit(solution)/shard_map/ppermute | solution.py:224
  9.2 1.3 %collective-permute-start.1 = (bf16[8,16,1024]{2,1,0:T(8,128)(2,1)}, bf16[8,16,1024]{2,1,0:T(8,128)(2,1)S(1)}, u32[]{:S(2)}, u32[]{:S(2)}) collective-permute-start(bf16[8,16,1024]{2,1,0:T(8,128)(2,1)} %param.7), channel_id=1, source_target_pairs={{32,0},{64,32},{96,64},{128,96},{160,128},{192,160},{224,192},{256... | collective-permute-start | bytes 786440 | tf_op jit(solution)/shard_map/ppermute | solution.py:225
  10.5 2.3 %collective-permute-done = bf16[8,16,1024]{2,1,0:T(8,128)(2,1)S(1)} collective-permute-done((bf16[8,16,1024]{2,1,0:T(8,128)(2,1)}, bf16[8,16,1024]{2,1,0:T(8,128)(2,1)S(1)}, u32[]{:S(2)}, u32[]{:S(2)}) %collective-permute-start) | collective-permute-done | bytes 262176 | tf_op jit(solution)/shard_map/ppermute | solution.py:224
  12.8 1.0 constant_dynamic-update-slice_fusion.1
  13.8 7.7 %collective-permute-done.1 = bf16[8,16,1024]{2,1,0:T(8,128)(2,1)S(1)} collective-permute-done((bf16[8,16,1024]{2,1,0:T(8,128)(2,1)}, bf16[8,16,1024]{2,1,0:T(8,128)(2,1)S(1)}, u32[]{:S(2)}, u32[]{:S(2)}) %collective-permute-start.1) | collective-permute-done | bytes 262176 | tf_op jit(solution)/shard_map/ppermute | solution.py:225
  21.6 73.7 %collective-permute-start.3 = (bf16[24,16,1024]{2,1,0:T(8,128)(2,1)S(1)}, bf16[24,16,1024]{2,1,0:T(8,128)(2,1)S(1)}, u32[]{:S(2)}, u32[]{:S(2)}) collective-permute-start(bf16[24,16,1024]{2,1,0:T(8,128)(2,1)S(1)} %constant_dynamic-update-slice_fusion.mid), channel_id=1, source_target_pairs={{1,0},{2,1},{3,2},{4,3},{5,4},{6,5},{7,6},{8,7},{9,8},{10,9},{11,1... | collective-permute-start | bytes 2359304 | tf_op jit(solution)/shard_map/ppermute | solution.py:225
  95.3 2.0 %collective-permute-start.2 = (bf16[24,16,1024]{2,1,0:T(8,128)(2,1)S(1)}, bf16[24,16,1024]{2,1,0:T(8,128)(2,1)S(1)}, u32[]{:S(2)}, u32[]{:S(2)}) collective-permute-start(bf16[24,16,1024]{2,1,0:T(8,128)(2,1)S(1)} %constant_dynamic-update-slice_fusion.mid), channel_id=1, source_target_pairs={{0,1},{1,2},{2,3},{3,4},{4,5},{5,6},{6,7},{7,8},{8,9},{9,10},{10,1... | collective-permute-start | bytes 2359304 | tf_op jit(solution)/shard_map/ppermute | solution.py:224
  97.2 0.0 copy-start.5
  97.2 0.8 copy_multiply_fusion
  98.1 0.0 copy-start.3
  98.1 0.1 pad_maximum_fusion.rows_ref
  98.3 0.0 copy-start.1
  98.3 0.0 copy-start.2
  98.3 1.5 %bias.1 = f32[5,4,128,512]{3,2,1,0:T(8,128)S(1)} custom-call(f32[2,4,20,128]{3,2,1,0:T(8,128)S(1)} %pad_maximum_fusion.rows_ref), custom_call_target="tpu_custom_call" | custom-call | flops 4000000 | bytes 6291456 | tf_op jit(solution)/shard_map/bias/pallas_call | solution.py:237
  99.8 0.0 copy-start
  99.8 2.3 %copy-done = f32[5,4,128,512]{3,2,1,0:T(8,128)} copy-done((f32[5,4,128,512]{3,2,1,0:T(8,128)}, f32[5,4,128,512]{3,2,1,0:T(8,128)S(1)}, u32[]{:S(2)}) %copy-start) | copy-done | bytes 5242904
  102.1 0.0 collective-permute-done.3.right
  102.1 4.0 %collective-permute-done.2.left = bf16[24,16,1024]{2,1,0:T(8,128)(2,1)S(1)} collective-permute-done((bf16[24,16,1024]{2,1,0:T(8,128)(2,1)S(1)}, bf16[24,16,1024]{2,1,0:T(8,128)(2,1)S(1)}, u32[]{:S(2)}, u32[]{:S(2)}) %collective-permute-start.2) | collective-permute-done | bytes 786464 | tf_op jit(solution)/shard_map/ppermute | solution.py:224
  106.1 0.0 copy-done.5
  106.1 0.0 copy-done.3
  106.1 0.0 copy-done.1
  106.1 0.0 copy-done.2
  106.2 0.0 copy-start.4
  106.2 1.6 %copy-done.4 = bf16[2,512,1024]{2,1,0:T(8,128)(2,1)S(1)} copy-done((bf16[2,512,1024]{2,1,0:T(8,128)(2,1)S(1)}, bf16[2,512,1024]{2,1,0:T(8,128)(2,1)}, u32[]{:S(2)}) %copy-start.4) | copy-done | bytes 2097176
  107.7 19.3 %layers.1 = bf16[8,16,1024]{2,1,0:T(8,128)(2,1)} custom-call(bf16[24,16,1024]{2,1,0:T(8,128)(2,1)S(1)} %collective-permute-done.2.left, bf16[24,16,1024]{2,1,0:T(8,128)(2,1)S(1)} %constant_dynamic-update-slice_fusion.mid, bf16[24,16,1024]{2,1,0:T(8,128)(2,1)S(1)} %collective-permute-done.3.right, f32[2,1024]{1,0:T(2,128)S(1)} %copy-done.5, ...), custom_call_target="tpu_custom_call" | custom-call | flops 6000000000 | bytes 16777216 | tf_op jit(solution)/shard_map/layers/pallas_call | solution.py:254
  (3 shorter events, 0.1 us)
Async XLA Ops:
  0.0 12.8 %collective-permute-start = (bf16[8,16,1024]{2,1,0:T(8,128)(2,1)}, bf16[8,16,1024]{2,1,0:T(8,128)(2,1)S(1)}, u32[]{:S(2)}, u32[]{:S(2)}) collective-permute-start(bf16[8,16,1024]{2,1,0:T(8,128)(2,1)} %param.7), channel_id=1, source_target_pairs={{0,32},{32,64},{64,96},{96,128},{128,160},{160,192},{192,224},{224... | collective-permute-start | bytes 786440 | tf_op jit(solution)/shard_map/ppermute | solution.py:224
  9.2 12.3 %collective-permute-start.1 = (bf16[8,16,1024]{2,1,0:T(8,128)(2,1)}, bf16[8,16,1024]{2,1,0:T(8,128)(2,1)S(1)}, u32[]{:S(2)}, u32[]{:S(2)}) collective-permute-start(bf16[8,16,1024]{2,1,0:T(8,128)(2,1)} %param.7), channel_id=1, source_target_pairs={{32,0},{64,32},{96,64},{128,96},{160,128},{192,160},{224,192},{256... | collective-permute-start | bytes 786440 | tf_op jit(solution)/shard_map/ppermute | solution.py:225
  21.6 80.6 %collective-permute-start.3 = (bf16[24,16,1024]{2,1,0:T(8,128)(2,1)S(1)}, bf16[24,16,1024]{2,1,0:T(8,128)(2,1)S(1)}, u32[]{:S(2)}, u32[]{:S(2)}) collective-permute-start(bf16[24,16,1024]{2,1,0:T(8,128)(2,1)S(1)} %constant_dynamic-update-slice_fusion.mid), channel_id=1, source_target_pairs={{1,0},{2,1},{3,2},{4,3},{5,4},{6,5},{7,6},{8,7},{9,8},{10,9},{11,1... | collective-permute-start | bytes 2359304 | tf_op jit(solution)/shard_map/ppermute | solution.py:225
  95.3 10.9 %collective-permute-start.2 = (bf16[24,16,1024]{2,1,0:T(8,128)(2,1)S(1)}, bf16[24,16,1024]{2,1,0:T(8,128)(2,1)S(1)}, u32[]{:S(2)}, u32[]{:S(2)}) collective-permute-start(bf16[24,16,1024]{2,1,0:T(8,128)(2,1)S(1)} %constant_dynamic-update-slice_fusion.mid), channel_id=1, source_target_pairs={{0,1},{1,2},{2,3},{3,4},{4,5},{5,6},{6,7},{7,8},{8,9},{9,10},{10,1... | collective-permute-start | bytes 2359304 | tf_op jit(solution)/shard_map/ppermute | solution.py:224
  97.2 8.9 %copy-start.5 = (f32[2,1024]{1,0:T(2,128)S(1)}, f32[2,1024]{1,0:T(2,128)}, u32[]{:S(2)}) copy-start(f32[2,1024]{1,0:T(2,128)} %gain.1) | copy-start | bytes 24580
  98.1 8.1 %copy-start.3 = (bf16[2,1024,512]{2,1,0:T(8,128)(2,1)S(1)}, bf16[2,1024,512]{2,1,0:T(8,128)(2,1)}, u32[]{:S(2)}) copy-start(bf16[2,1024,512]{2,1,0:T(8,128)(2,1)} %w_value.1) | copy-start | bytes 6291460
  98.3 7.9 %copy-start.1 = (bf16[2,1024,512]{2,1,0:T(8,128)(2,1)S(1)}, bf16[2,1024,512]{2,1,0:T(8,128)(2,1)}, u32[]{:S(2)}) copy-start(bf16[2,1024,512]{2,1,0:T(8,128)(2,1)} %w_query.1) | copy-start | bytes 6291460
  98.3 7.8 %copy-start.2 = (bf16[2,1024,512]{2,1,0:T(8,128)(2,1)S(1)}, bf16[2,1024,512]{2,1,0:T(8,128)(2,1)}, u32[]{:S(2)}) copy-start(bf16[2,1024,512]{2,1,0:T(8,128)(2,1)} %w_key.1) | copy-start | bytes 6291460
  99.8 2.3 %copy-start = (f32[5,4,128,512]{3,2,1,0:T(8,128)}, f32[5,4,128,512]{3,2,1,0:T(8,128)S(1)}, u32[]{:S(2)}) copy-start(f32[5,4,128,512]{3,2,1,0:T(8,128)S(1)} %bias.1) | copy-start | bytes 15728644
  106.2 1.6 %copy-start.4 = (bf16[2,512,1024]{2,1,0:T(8,128)(2,1)S(1)}, bf16[2,512,1024]{2,1,0:T(8,128)(2,1)}, u32[]{:S(2)}) copy-start(bf16[2,512,1024]{2,1,0:T(8,128)(2,1)} %w_out.1) | copy-start | bytes 6291460

commit v2 on v1

v2 whole, which is shorter than its diff:
```python
import functools
import math

import jax
import jax.numpy as jnp
from jax import lax
from jax.experimental import pallas as pl
from jax.experimental.pallas import tpu as pltpu
from jax.sharding import PartitionSpec as P

HEAD_DIM = 128
WIN_ROWS = 8
WIN_COLS = 16
LAYERS = 2
HALF_ROWS = WIN_ROWS // 2
HALF_COLS = WIN_COLS // 2

NORM_EPSILON = 1e-06
LOG2E = math.log2(math.e)
MASKED = -1e30

BLOCK_ROWS = 8
BLOCK_COLS = 16
SLAB_ROWS = BLOCK_ROWS + WIN_ROWS
SLAB_COLS = BLOCK_COLS + WIN_COLS
QUERIES = BLOCK_ROWS * BLOCK_COLS
SLAB = SLAB_ROWS * SLAB_COLS
LANES = 128
GROUP = LANES // SLAB_COLS
SPAN = SLAB_ROWS - GROUP + BLOCK_ROWS
BLOCKS = 5

TILES = 3
SLOTS = 3
CHUNK = 32

ORDER = ((0, -1), (-1, 0), (-1, -1), (-1, 1), (1, -1), (0, 1), (1, 0), (1, 1))

VMEM = pl.BlockSpec(memory_space=pltpu.VMEM)


def bias_rows(table):
    rows = jnp.transpose(table * LOG2E, (0, 2, 1, 3))
    after = SPAN + GROUP - 1 - HALF_ROWS - rows.shape[1]
    return jnp.pad(rows, ((0, 0), (HALF_ROWS, after), (0, 0), (0, LANES - rows.shape[3])))


def bias_kernel(grid_rows, grid_cols, tile_rows, tile_cols, rows_ref, out_ref, shifted):
    layers, _, heads = rows_ref.shape[:3]
    first_row = lax.axis_index("sp") * tile_rows
    first_col = lax.axis_index("tp") * tile_cols

    for layer in range(layers):
        for u in range(SPAN):
            lines = rows_ref[layer, u]
            for g in range(1, GROUP):
                lines = lines + pltpu.roll(rows_ref[layer, u + g], g * SLAB_COLS, 1)
            for head in range(heads):
                shifted[layer, head, u] = pltpu.roll(
                    jnp.broadcast_to(lines[head : head + 1], (BLOCK_COLS, LANES)),
                    LANES - (HALF_COLS - 1),
                    1,
                    stride=1,
                    stride_axis=0,
                )

    lane = lax.broadcasted_iota(jnp.int32, (BLOCK_COLS, LANES), 1)
    column = lax.broadcasted_iota(jnp.int32, (BLOCK_COLS, LANES), 0)
    key_col = lane % SLAB_COLS
    key_row = lane // SLAB_COLS

    def block(index, _):
        last = index // (BLOCKS - 1)
        row_block, col_block = (index // 2) % 2, index % 2
        row0 = first_row + (1 - last) * (row_block * BLOCK_ROWS - HALF_ROWS)
        col0 = first_col + (1 - last) * (col_block * BLOCK_COLS - HALF_COLS)
        col_start = jnp.clip(col0 + column - HALF_COLS, 0, grid_cols - WIN_COLS)
        behind = col0 - HALF_COLS + key_col - col_start
        col_inside = (behind >= 0) & (behind < WIN_COLS)
        for i in range(BLOCK_ROWS):
            row_start = jnp.clip(row0 + i - HALF_ROWS, 0, grid_rows - WIN_ROWS)
            for j in range(SLAB_ROWS // GROUP):
                below = key_row + (row0 - HALF_ROWS + j * GROUP - row_start)
                inside = col_inside & (below >= 0) & (below < WIN_ROWS)
                for head in range(heads):
                    out_ref[
                        index,
                        head,
                        i * BLOCK_COLS : (i + 1) * BLOCK_COLS,
                        j * LANES : (j + 1) * LANES,
                    ] = jnp.where(
                        inside, shifted[last, head, GROUP * j - i + BLOCK_ROWS - 1], MASKED
                    )
        return 0

    lax.fori_loop(0, BLOCKS, block, 0)


def normed_rows(values, gain):
    factor = lax.rsqrt(jnp.mean(values * values, axis=-1, keepdims=True) + NORM_EPSILON)
    return values * factor * gain


def project(cells, weight):
    rows, cols, width = cells.shape
    out = jnp.dot(
        cells.reshape(rows * cols, width), weight, preferred_element_type=jnp.float32
    )
    return out.astype(jnp.bfloat16).reshape(rows, cols, weight.shape[1])


def layers_kernel(*refs):
    tiles, refs = refs[: TILES * TILES], refs[TILES * TILES :]
    gain, w_query, w_key, w_value, w_out, bias, out_ref = refs[:7]
    normed, normed_q, keys, values, queries, mixture, branch, center, scores, weights = refs[7:]
    f32, bf16 = jnp.float32, jnp.bfloat16
    heads = w_query.shape[2] // HEAD_DIM
    rows, cols = normed.shape[:2]
    region_rows, region_cols = mixture.shape[:2]
    slots = scores.shape[0]

    def put_values(where, out):
        for head in range(heads):
            values[(*where, pl.ds(2 * head * HEAD_DIM, HEAD_DIM))] = out[
                :, :, head * HEAD_DIM : (head + 1) * HEAD_DIM
            ]

    def attend(units):
        def products(step):
            _, head, tile, slab = units[step]
            lanes = pl.ds(head * HEAD_DIM, HEAD_DIM)
            scores[step % slots] = lax.dot_general(
                queries[(*tile, lanes)].reshape(QUERIES, HEAD_DIM),
                keys[(*slab, lanes)].reshape(SLAB, HEAD_DIM),
                (((1,), (1,)), ((), ())),
                preferred_element_type=f32,
            )

        def softmax(step):
            block, head, _, _ = units[step]
            for first in range(0, QUERIES, CHUNK):
                part = pl.ds(first, CHUNK)
                shifted = scores[step % slots, part] * (LOG2E / HEAD_DIM**0.5)
                shifted = shifted + bias[block, head, part]
                top = jnp.max(shifted, axis=1, keepdims=True)
                weights[step % slots, part] = jnp.exp2(shifted - top).astype(bf16)

        def mix(step):
            _, head, tile, slab = units[step]
            both = jnp.dot(
                weights[step % slots],
                values[(*slab, pl.ds(2 * head * HEAD_DIM, 2 * HEAD_DIM))].reshape(
                    SLAB, 2 * HEAD_DIM
                ),
                preferred_element_type=f32,
            )
            out = (both[:, :HEAD_DIM] / both[:, HEAD_DIM:]).astype(bf16)
            mixture[(*tile, pl.ds(head * HEAD_DIM, HEAD_DIM))] = out.reshape(
                BLOCK_ROWS, BLOCK_COLS, HEAD_DIM
            )

        for step in range(len(units) + 2):
            if step < len(units):
                products(step)
            if 0 <= step - 1 < len(units):
                softmax(step - 1)
            if 0 <= step - 2:
                mix(step - 2)

    def part_of(r, c):
        return tiles[r // BLOCK_ROWS * TILES + c][r % BLOCK_ROWS].astype(f32)

    for head in range(heads):
        values[:, :, pl.ds((2 * head + 1) * HEAD_DIM, HEAD_DIM)] = jnp.ones(
            (rows, cols, HEAD_DIM), bf16
        )
    for r in range(rows):
        parts = [normed_rows(part_of(r, c), gain[0:1]) for c in range(TILES)]
        for index, part in enumerate(parts):
            normed[r, index * BLOCK_COLS : (index + 1) * BLOCK_COLS] = part.astype(bf16)
        if 0 <= r - HALF_ROWS < region_rows:
            for index in range(2):
                both = (parts[index][HALF_COLS:], parts[index + 1][:HALF_COLS])
                normed_q[r - HALF_ROWS, index * BLOCK_COLS : (index + 1) * BLOCK_COLS] = (
                    jnp.concatenate(both, axis=0).astype(bf16)
                )
        if r % BLOCK_ROWS == BLOCK_ROWS - 1:
            band = pl.ds(r + 1 - BLOCK_ROWS, BLOCK_ROWS)
            keys[band] = project(normed[band], w_key[0])
            put_values((band, slice(None)), project(normed[band], w_value[0]))
    queries[...] = project(normed_q[...], w_query[0])

    units = []
    for index in range(BLOCKS - 1):
        row, col = index // 2 * BLOCK_ROWS, index % 2 * BLOCK_COLS
        tile = (pl.ds(row, BLOCK_ROWS), pl.ds(col, BLOCK_COLS))
        slab = (pl.ds(row, SLAB_ROWS), pl.ds(col, SLAB_COLS))
        units += [(index, head, tile, slab) for head in range(heads)]
    attend(units)
    branch[...] = jnp.dot(
        mixture[...].reshape(region_rows * region_cols, heads * HEAD_DIM),
        w_out[0],
        preferred_element_type=f32,
    ).reshape(branch.shape)

    own = pl.ds(HALF_ROWS, BLOCK_ROWS)
    inner = slice(HALF_COLS, HALF_COLS + BLOCK_COLS)
    for r in range(region_rows):
        before, here, after = (part_of(r + HALF_ROWS, c) for c in range(TILES))
        tokens = jnp.concatenate((before[HALF_COLS:], here, after[:HALF_COLS]), axis=0)
        stream = (tokens + branch[r]).astype(bf16).astype(f32)
        part = normed_rows(stream, gain[1:2])
        normed[r, :region_cols] = part.astype(bf16)
        if 0 <= r - HALF_ROWS < BLOCK_ROWS:
            normed_q[r - HALF_ROWS, :BLOCK_COLS] = part[inner].astype(bf16)
            center[r - HALF_ROWS] = stream[inner]
    region = (pl.ds(0, region_rows), pl.ds(0, region_cols))
    tile = (pl.ds(0, BLOCK_ROWS), pl.ds(0, BLOCK_COLS))
    keys[region] = project(normed[region], w_key[1])
    put_values(region, project(normed[region], w_value[1]))
    queries[tile] = project(normed_q[tile], w_query[1])
    attend([(BLOCKS - 1, head, tile, region) for head in range(heads)])
    last = jnp.dot(
        mixture[tile].reshape(QUERIES, heads * HEAD_DIM), w_out[1], preferred_element_type=f32
    )
    out_ref[...] = (center[...] + last.reshape(out_ref.shape)).astype(out_ref.dtype)


def from_offset(cells, row, col):
    rows, cols = lax.axis_size("sp"), lax.axis_size("tp")
    pairs = [
        ((r + row) * cols + c + col, r * cols + c)
        for r in range(rows)
        for c in range(cols)
        if 0 <= r + row < rows and 0 <= c + col < cols
    ]
    return lax.ppermute(cells, ("sp", "tp"), pairs)


def on_device(grid_tokens, norm_gain, w_query, w_key, w_value, offset_bias, w_out):
    tile_rows, tile_cols, width = grid_tokens.shape
    grid_rows = tile_rows * lax.axis_size("sp")
    grid_cols = tile_cols * lax.axis_size("tp")
    heads = offset_bias.shape[1]
    inner = heads * HEAD_DIM
    bf16, f32 = jnp.bfloat16, jnp.float32

    bias = pl.pallas_call(
        functools.partial(bias_kernel, grid_rows, grid_cols, tile_rows, tile_cols),
        out_shape=jax.ShapeDtypeStruct((BLOCKS, heads, QUERIES, SLAB), f32),
        in_specs=[VMEM],
        out_specs=VMEM,
        scratch_shapes=[pltpu.VMEM((LAYERS, heads, SPAN, BLOCK_COLS, LANES), f32)],
        compiler_params=pltpu.CompilerParams(vmem_limit_bytes=8 * 2**20),
        cost_estimate=pl.CostEstimate(flops=4 * 10**6, bytes_accessed=6 * 2**20, transcendentals=0),
        name="bias",
    )(bias_rows(offset_bias))

    arrived = {(0, 0): grid_tokens}
    for offset in ORDER:
        arrived[offset] = from_offset(grid_tokens, *offset)
    tiles = [arrived[(row, col)] for row in (-1, 0, 1) for col in (-1, 0, 1)]

    rows, cols = TILES * tile_rows, TILES * tile_cols
    region_rows, region_cols = 2 * tile_rows, 2 * tile_cols
    return pl.pallas_call(
        layers_kernel,
        out_shape=jax.ShapeDtypeStruct(grid_tokens.shape, grid_tokens.dtype),
        in_specs=[VMEM] * (len(tiles) + 6),
        out_specs=VMEM,
        scratch_shapes=[
            pltpu.VMEM((rows, cols, width), bf16),
            pltpu.VMEM((region_rows, region_cols, width), bf16),
            pltpu.VMEM((rows, cols, inner), bf16),
            pltpu.VMEM((rows, cols, 2 * inner), bf16),
            pltpu.VMEM((region_rows, region_cols, inner), bf16),
            pltpu.VMEM((region_rows, region_cols, inner), bf16),
            pltpu.VMEM((region_rows, region_cols, width), f32),
            pltpu.VMEM((tile_rows, tile_cols, width), f32),
            pltpu.VMEM((SLOTS, QUERIES, SLAB), f32),
            pltpu.VMEM((SLOTS, QUERIES, SLAB), bf16),
        ],
        compiler_params=pltpu.CompilerParams(vmem_limit_bytes=24 * 2**20),
        cost_estimate=pl.CostEstimate(
            flops=6 * 10**9, bytes_accessed=16 * 2**20, transcendentals=10**6
        ),
        name="layers",
    )(*tiles, norm_gain, w_query, w_key, w_value, w_out, bias)


def solution(mesh):
    return jax.shard_map(
        on_device,
        mesh=mesh,
        in_specs=(P(("grp", "sp"), "tp", None), P(), P(), P(), P(), P(), P()),
        out_specs=P(("grp", "sp"), "tp", None),
        check_vma=False,
    )
```

time: 127 us -> 121 us (0.953)
  starting transfers between devices: 86.2 us -> 98.9 us
  Pallas kernels: 20.8 us -> 11.6 us
  waiting for transfers between devices: 14 us -> 5.38 us
  local copies, waits for them, and re-layouts: 4.94 us -> 3.22 us
    ppermute x4 -> x8, starting transfers between devices: 86.2 us -> 98.9 us  [from_offset(): return lax.ppermute(cells, ('sp', 'tp'), pairs)]
    pallas_call x1, Pallas kernels: 19.3 us -> 8.54 us  [on_device(): pl.pallas_call(layers_kernel, out_shape=jax.ShapeDtypeStruct(grid_tokens....]
    ppermute x4 -> x8, waiting for transfers between devices: 14 us -> 5.38 us  [from_offset(): return lax.ppermute(cells, ('sp', 'tp'), pairs)]
    unnamed x14 -> x12, local copies, waits for them, and re-layouts: 4.89 us -> 3.2 us
    pallas_call x1, Pallas kernels: 1.5 us -> 3.1 us  [on_device(): pl.pallas_call(functools.partial(bias_kernel, grid_rows, grid_cols, tile_...]
  transfers between devices with their start and end apart: 4 -> 8, of which waited for: 3 -> 1; matrix products, arithmetic and copies ran while one was open for 2% -> 1% of each run, Pallas kernels for 1% -> 3%
where the time goes in v2:
time: 121 us; the launch traced here: 120 us
  starting transfers between devices  98.9 us (82%)
  Pallas kernels  11.6 us (10%)
  waiting for transfers between devices  5.38 us (4%)
  local copies, waits for them, and re-layouts  3.22 us (3%)
    ppermute x8, starting transfers between devices, from_offset(): return lax.ppermute(cells, ('sp', 'tp'), pairs)  98.9 us
    pallas_call x1, Pallas kernels, on_device(): pl.pallas_call(layers_kernel, out_shape=jax.ShapeDtypeStruct(grid_tokens....  8.54 us
    ppermute x8, waiting for transfers between devices, from_offset(): return lax.ppermute(cells, ('sp', 'tp'), pairs)  5.38 us
    unnamed x12, local copies, waits for them, and re-layouts  3.2 us
    pallas_call x1, Pallas kernels, on_device(): pl.pallas_call(functools.partial(bias_kernel, grid_rows, grid_cols, tile_...  3.1 us
  transfers between devices with their start and end apart: 8, of which 1 were waited for; matrix products, arithmetic and copies ran while one was open for 1% of the time, Pallas kernels for 3%

profile of v2, /device:TPU:5, one launch (start us, length us, event | category | flops | bytes accessed | tf_op | source)
XLA Modules:
  0.0 120.2 jit_solution(5398609268085020202)
XLA Ops:
  0.0 1.3 %collective-permute-start.6 = (bf16[8,16,1024]{2,1,0:T(8,128)(2,1)}, bf16[8,16,1024]{2,1,0:T(8,128)(2,1)S(1)}, u32[]{:S(2)}, u32[]{:S(2)}) collective-permute-start(bf16[8,16,1024]{2,1,0:T(8,128)(2,1)} %refs_4_.1), channel_id=1, source_target_pairs={{32,0},{33,1},{34,2},{35,3},{36,4},{37,5},{38,6},{39,7},{40,8},{41... | collective-permute-start | bytes 786440 | tf_op jit(solution)/shard_map/ppermute | solution.py:237
  1.3 1.3 %collective-permute-start.5 = (bf16[8,16,1024]{2,1,0:T(8,128)(2,1)}, bf16[8,16,1024]{2,1,0:T(8,128)(2,1)S(1)}, u32[]{:S(2)}, u32[]{:S(2)}) collective-permute-start(bf16[8,16,1024]{2,1,0:T(8,128)(2,1)} %refs_4_.1), channel_id=1, source_target_pairs={{32,1},{33,2},{34,3},{35,4},{36,5},{37,6},{38,7},{39,8},{40,9},{41... | collective-permute-start | bytes 786440 | tf_op jit(solution)/shard_map/ppermute | solution.py:237
  2.6 84.8 %collective-permute-start.4 = (bf16[8,16,1024]{2,1,0:T(8,128)(2,1)}, bf16[8,16,1024]{2,1,0:T(8,128)(2,1)S(1)}, u32[]{:S(2)}, u32[]{:S(2)}) collective-permute-start(bf16[8,16,1024]{2,1,0:T(8,128)(2,1)} %refs_4_.1), channel_id=1, source_target_pairs={{1,0},{2,1},{3,2},{4,3},{5,4},{6,5},{7,6},{8,7},{9,8},{10,9},{11,1... | collective-permute-start | bytes 786440 | tf_op jit(solution)/shard_map/ppermute | solution.py:237
  87.4 2.0 %collective-permute-start.3 = (bf16[8,16,1024]{2,1,0:T(8,128)(2,1)}, bf16[8,16,1024]{2,1,0:T(8,128)(2,1)S(1)}, u32[]{:S(2)}, u32[]{:S(2)}) collective-permute-start(bf16[8,16,1024]{2,1,0:T(8,128)(2,1)} %refs_4_.1), channel_id=1, source_target_pairs={{0,1},{1,2},{2,3},{3,4},{4,5},{5,6},{6,7},{7,8},{8,9},{9,10},{10,1... | collective-permute-start | bytes 786440 | tf_op jit(solution)/shard_map/ppermute | solution.py:237
  89.4 5.4 %collective-permute-start.2 = (bf16[8,16,1024]{2,1,0:T(8,128)(2,1)}, bf16[8,16,1024]{2,1,0:T(8,128)(2,1)S(1)}, u32[]{:S(2)}, u32[]{:S(2)}) collective-permute-start(bf16[8,16,1024]{2,1,0:T(8,128)(2,1)} %refs_4_.1), channel_id=1, source_target_pairs={{1,32},{2,33},{3,34},{4,35},{5,36},{6,37},{7,38},{8,39},{9,40},{10... | collective-permute-start | bytes 786440 | tf_op jit(solution)/shard_map/ppermute | solution.py:237
  94.7 0.0 collective-permute-done.6.refs_7_
  94.8 1.6 %collective-permute-start.1 = (bf16[8,16,1024]{2,1,0:T(8,128)(2,1)}, bf16[8,16,1024]{2,1,0:T(8,128)(2,1)S(1)}, u32[]{:S(2)}, u32[]{:S(2)}) collective-permute-start(bf16[8,16,1024]{2,1,0:T(8,128)(2,1)} %refs_4_.1), channel_id=1, source_target_pairs={{0,32},{1,33},{2,34},{3,35},{4,36},{5,37},{6,38},{7,39},{8,40},{9,... | collective-permute-start | bytes 786440 | tf_op jit(solution)/shard_map/ppermute | solution.py:237
  96.3 0.0 collective-permute-done.5.refs_6_
  96.3 1.3 %collective-permute-start = (bf16[8,16,1024]{2,1,0:T(8,128)(2,1)}, bf16[8,16,1024]{2,1,0:T(8,128)(2,1)S(1)}, u32[]{:S(2)}, u32[]{:S(2)}) collective-permute-start(bf16[8,16,1024]{2,1,0:T(8,128)(2,1)} %refs_4_.1), channel_id=1, source_target_pairs={{0,33},{1,34},{2,35},{3,36},{4,37},{5,38},{6,39},{7,40},{8,41},{9,... | collective-permute-start | bytes 786440 | tf_op jit(solution)/shard_map/ppermute | solution.py:237
  97.7 0.0 collective-permute-done.4.refs_5_
  97.7 1.3 %collective-permute-start.7 = (bf16[8,16,1024]{2,1,0:T(8,128)(2,1)}, bf16[8,16,1024]{2,1,0:T(8,128)(2,1)S(1)}, u32[]{:S(2)}, u32[]{:S(2)}) collective-permute-start(bf16[8,16,1024]{2,1,0:T(8,128)(2,1)} %refs_4_.1), channel_id=1, source_target_pairs={{33,0},{34,1},{35,2},{36,3},{37,4},{38,5},{39,6},{40,7},{41,8},{42... | collective-permute-start | bytes 786440 | tf_op jit(solution)/shard_map/ppermute | solution.py:237
  99.0 0.8 multiply_bitcast_fusion
  99.9 0.0 copy-start
  99.9 0.0 copy-start.1
  99.9 0.0 copy-start.4
  99.9 0.0 copy-start.5
  99.9 3.1 %bias.1.refs_14_ = f32[5,4,128,512]{3,2,1,0:T(8,128)S(1)} custom-call(f32[2,23,4,128]{3,2,1,0:T(4,128)S(1)} %pad.4.rows_ref), custom_call_target="tpu_custom_call" | custom-call | flops 4000000 | bytes 6291456 | tf_op jit(solution)/shard_map/bias/pallas_call | solution.py:248
  103.0 0.0 collective-permute-done.3.refs_3_
  103.0 0.0 collective-permute-done.2.refs_2_
  103.0 5.4 %collective-permute-done.1.refs_1_ = bf16[8,16,1024]{2,1,0:T(8,128)(2,1)S(1)} collective-permute-done((bf16[8,16,1024]{2,1,0:T(8,128)(2,1)}, bf16[8,16,1024]{2,1,0:T(8,128)(2,1)S(1)}, u32[]{:S(2)}, u32[]{:S(2)}) %collective-permute-start.1) | collective-permute-done | bytes 262176 | tf_op jit(solution)/shard_map/ppermute | solution.py:237
  108.4 0.0 collective-permute-done.refs_0_
  108.4 0.0 collective-permute-done.7.refs_8_
  108.4 0.0 copy-done
  108.4 0.0 copy-done.1
  108.4 0.0 copy-done.4
  108.4 0.0 copy-done.5
  108.4 0.0 copy-start.2
  108.5 1.6 %copy-done.2 = bf16[2,1024,512]{2,1,0:T(8,128)(2,1)S(1)} copy-done((bf16[2,1024,512]{2,1,0:T(8,128)(2,1)S(1)}, bf16[2,1024,512]{2,1,0:T(8,128)(2,1)}, u32[]{:S(2)}) %copy-start.2) | copy-done | bytes 2097176
  110.0 0.0 copy-start.3
  110.0 1.6 %copy-done.3 = bf16[2,512,1024]{2,1,0:T(8,128)(2,1)S(1)} copy-done((bf16[2,512,1024]{2,1,0:T(8,128)(2,1)S(1)}, bf16[2,512,1024]{2,1,0:T(8,128)(2,1)}, u32[]{:S(2)}) %copy-start.3) | copy-done | bytes 2097176
  111.6 8.5 %layers.1 = bf16[8,16,1024]{2,1,0:T(8,128)(2,1)} custom-call(bf16[8,16,1024]{2,1,0:T(8,128)(2,1)S(1)} %collective-permute-done.refs_0_, bf16[8,16,1024]{2,1,0:T(8,128)(2,1)S(1)} %collective-permute-done.1.refs_1_, bf16[8,16,1024]{2,1,0:T(8,128)(2,1)S(1)} %collective-permute-done.2.refs_2_, bf16[8,16,1024]{2,1,0:T(8,128)(2,1)S(1)} %collective-permute-done.3.refs_3_, ...), custom_call_target="tpu_custom_call" | custom-call | flops 6000000000 | bytes 16777216 | tf_op jit(solution)/shard_map/layers/pallas_call | solution.py:266
  (1 shorter events, 0.0 us)
Async XLA Ops:
  0.0 94.8 %collective-permute-start.6 = (bf16[8,16,1024]{2,1,0:T(8,128)(2,1)}, bf16[8,16,1024]{2,1,0:T(8,128)(2,1)S(1)}, u32[]{:S(2)}, u32[]{:S(2)}) collective-permute-start(bf16[8,16,1024]{2,1,0:T(8,128)(2,1)} %refs_4_.1), channel_id=1, source_target_pairs={{32,0},{33,1},{34,2},{35,3},{36,4},{37,5},{38,6},{39,7},{40,8},{41... | collective-permute-start | bytes 786440 | tf_op jit(solution)/shard_map/ppermute | solution.py:237
  1.3 95.0 %collective-permute-start.5 = (bf16[8,16,1024]{2,1,0:T(8,128)(2,1)}, bf16[8,16,1024]{2,1,0:T(8,128)(2,1)S(1)}, u32[]{:S(2)}, u32[]{:S(2)}) collective-permute-start(bf16[8,16,1024]{2,1,0:T(8,128)(2,1)} %refs_4_.1), channel_id=1, source_target_pairs={{32,1},{33,2},{34,3},{35,4},{36,5},{37,6},{38,7},{39,8},{40,9},{41... | collective-permute-start | bytes 786440 | tf_op jit(solution)/shard_map/ppermute | solution.py:237
  2.6 95.0 %collective-permute-start.4 = (bf16[8,16,1024]{2,1,0:T(8,128)(2,1)}, bf16[8,16,1024]{2,1,0:T(8,128)(2,1)S(1)}, u32[]{:S(2)}, u32[]{:S(2)}) collective-permute-start(bf16[8,16,1024]{2,1,0:T(8,128)(2,1)} %refs_4_.1), channel_id=1, source_target_pairs={{1,0},{2,1},{3,2},{4,3},{5,4},{6,5},{7,6},{8,7},{9,8},{10,9},{11,1... | collective-permute-start | bytes 786440 | tf_op jit(solution)/shard_map/ppermute | solution.py:237
  87.4 15.6 %collective-permute-start.3 = (bf16[8,16,1024]{2,1,0:T(8,128)(2,1)}, bf16[8,16,1024]{2,1,0:T(8,128)(2,1)S(1)}, u32[]{:S(2)}, u32[]{:S(2)}) collective-permute-start(bf16[8,16,1024]{2,1,0:T(8,128)(2,1)} %refs_4_.1), channel_id=1, source_target_pairs={{0,1},{1,2},{2,3},{3,4},{4,5},{5,6},{6,7},{7,8},{8,9},{9,10},{10,1... | collective-permute-start | bytes 786440 | tf_op jit(solution)/shard_map/ppermute | solution.py:237
  89.4 13.7 %collective-permute-start.2 = (bf16[8,16,1024]{2,1,0:T(8,128)(2,1)}, bf16[8,16,1024]{2,1,0:T(8,128)(2,1)S(1)}, u32[]{:S(2)}, u32[]{:S(2)}) collective-permute-start(bf16[8,16,1024]{2,1,0:T(8,128)(2,1)} %refs_4_.1), channel_id=1, source_target_pairs={{1,32},{2,33},{3,34},{4,35},{5,36},{6,37},{7,38},{8,39},{9,40},{10... | collective-permute-start | bytes 786440 | tf_op jit(solution)/shard_map/ppermute | solution.py:237
  94.8 13.6 %collective-permute-start.1 = (bf16[8,16,1024]{2,1,0:T(8,128)(2,1)}, bf16[8,16,1024]{2,1,0:T(8,128)(2,1)S(1)}, u32[]{:S(2)}, u32[]{:S(2)}) collective-permute-start(bf16[8,16,1024]{2,1,0:T(8,128)(2,1)} %refs_4_.1), channel_id=1, source_target_pairs={{0,32},{1,33},{2,34},{3,35},{4,36},{5,37},{6,38},{7,39},{8,40},{9,... | collective-permute-start | bytes 786440 | tf_op jit(solution)/shard_map/ppermute | solution.py:237
  96.3 12.1 %collective-permute-start = (bf16[8,16,1024]{2,1,0:T(8,128)(2,1)}, bf16[8,16,1024]{2,1,0:T(8,128)(2,1)S(1)}, u32[]{:S(2)}, u32[]{:S(2)}) collective-permute-start(bf16[8,16,1024]{2,1,0:T(8,128)(2,1)} %refs_4_.1), channel_id=1, source_target_pairs={{0,33},{1,34},{2,35},{3,36},{4,37},{5,38},{6,39},{7,40},{8,41},{9,... | collective-permute-start | bytes 786440 | tf_op jit(solution)/shard_map/ppermute | solution.py:237
  97.7 10.7 %collective-permute-start.7 = (bf16[8,16,1024]{2,1,0:T(8,128)(2,1)}, bf16[8,16,1024]{2,1,0:T(8,128)(2,1)S(1)}, u32[]{:S(2)}, u32[]{:S(2)}) collective-permute-start(bf16[8,16,1024]{2,1,0:T(8,128)(2,1)} %refs_4_.1), channel_id=1, source_target_pairs={{33,0},{34,1},{35,2},{36,3},{37,4},{38,5},{39,6},{40,7},{41,8},{42... | collective-permute-start | bytes 786440 | tf_op jit(solution)/shard_map/ppermute | solution.py:237
  99.9 8.5 %copy-start = (bf16[2,1024,512]{2,1,0:T(8,128)(2,1)S(1)}, bf16[2,1024,512]{2,1,0:T(8,128)(2,1)}, u32[]{:S(2)}) copy-start(bf16[2,1024,512]{2,1,0:T(8,128)(2,1)} %refs_10_.1) | copy-start | bytes 6291460
  99.9 8.5 %copy-start.1 = (bf16[2,1024,512]{2,1,0:T(8,128)(2,1)S(1)}, bf16[2,1024,512]{2,1,0:T(8,128)(2,1)}, u32[]{:S(2)}) copy-start(bf16[2,1024,512]{2,1,0:T(8,128)(2,1)} %refs_11_.1) | copy-start | bytes 6291460
  99.9 8.5 %copy-start.4 = (bf16[8,16,1024]{2,1,0:T(8,128)(2,1)S(1)}, bf16[8,16,1024]{2,1,0:T(8,128)(2,1)}, u32[]{:S(2)}) copy-start(bf16[8,16,1024]{2,1,0:T(8,128)(2,1)} %refs_4_.1) | copy-start | bytes 786436
  99.9 8.5 %copy-start.5 = (f32[2,1024]{1,0:T(2,128)S(1)}, f32[2,1024]{1,0:T(2,128)}, u32[]{:S(2)}) copy-start(f32[2,1024]{1,0:T(2,128)} %refs_9_.1) | copy-start | bytes 24580
  108.4 1.6 %copy-start.2 = (bf16[2,1024,512]{2,1,0:T(8,128)(2,1)S(1)}, bf16[2,1024,512]{2,1,0:T(8,128)(2,1)}, u32[]{:S(2)}) copy-start(bf16[2,1024,512]{2,1,0:T(8,128)(2,1)} %refs_12_.1) | copy-start | bytes 6291460
  110.0 1.6 %copy-start.3 = (bf16[2,512,1024]{2,1,0:T(8,128)(2,1)S(1)}, bf16[2,512,1024]{2,1,0:T(8,128)(2,1)}, u32[]{:S(2)}) copy-start(bf16[2,512,1024]{2,1,0:T(8,128)(2,1)} %refs_13_.1) | copy-start | bytes 6291460
